TPU v7x, 32 devices: a whole 2x2x4 slice. The times are simulated.
32 devices in a mesh: sp: 2 (over x), dp: 16 (over z, y, core).
Axes of the slice: x: 2, y: 2, z: 4, core: 2. Of those that a mesh axis runs over, the one named last changes fastest.
Arguments:
- queries: bfloat16 [16, 384, 16, 128], P('dp', 'sp'), may hold values from -6 to 6
- keys: bfloat16 [16, 384, 16, 128], P('dp', 'sp'), may hold values from -6 to 6
- values: bfloat16 [16, 384, 16, 128], P('dp', 'sp'), may hold values from -6 to 6
- mix_ratio: float32 [16], replicated, may hold values from 0.3 to 0.8
- out_gain: float32 [128], replicated, may hold values from 0.1 to 1.9
- out_weight: bfloat16 [2048, 2048], P(None, 'dp'), may hold values from -0.125 to 0.125
Outputs:
- layer_out: bfloat16 [16, 384, 2048], P('dp', 'sp')
All inputs are finite; a program needn't handle non-finite values.
Results may differ from a plain program's by a relative error of at most 0.0098.
Values may be sent and summed in bfloat16 or wider, within the bound.
A program may use at most 64 MiB of HBM per device.

v0:
```python
import math
import jax
import jax.numpy as jnp
from jax import lax
from jax.sharding import PartitionSpec as P

theta_base = 500000.0
neg_large = -1e30
norm_eps = 1e-05


def rotate_halves(field, positions):
    width = field.shape[-1] // 2
    half = width // 2
    freqs = theta_base ** (-jnp.arange(half, dtype=jnp.float32) * 2.0 / width)
    angle = positions.astype(jnp.float32)[:, None] * freqs[None, :]
    cosine = jnp.cos(angle)[:, None, :]
    sine = jnp.sin(angle)[:, None, :]
    parts = field.reshape(field.shape[0], 2, width)
    lower = parts[..., :half]
    upper = parts[..., half:]
    turned = jnp.concatenate(
        [lower * cosine - upper * sine, upper * cosine + lower * sine], axis=-1
    )
    return turned.reshape(field.shape)


def masked_softmax(scores, visible):
    kept = jnp.where(visible, scores, neg_large)
    highest = jnp.max(kept, axis=-1, keepdims=True)
    powers = jnp.exp(kept - highest)
    return powers / jnp.sum(powers, axis=-1, keepdims=True)


def head_attention(query_head, key_head, value_head, ratio, gain):
    length = query_head.shape[0]
    width = query_head.shape[1] // 2
    positions = jnp.arange(length, dtype=jnp.int32)
    rotated_queries = (
        rotate_halves(query_head.astype(jnp.float32), positions) * width ** (-0.5)
    ).astype(jnp.bfloat16)
    rotated_keys = rotate_halves(key_head.astype(jnp.float32), positions).astype(jnp.bfloat16)
    block = math.gcd(512, length)

    def one_block(start):
        query_rows = lax.dynamic_slice_in_dim(rotated_queries, start, block, 0)
        visible = (start + jnp.arange(block, dtype=jnp.int32))[:, None] >= positions[None, :]
        first = jnp.dot(
            query_rows[:, :width], rotated_keys[:, :width].T, preferred_element_type=jnp.float32
        )
        second = jnp.dot(
            query_rows[:, width:], rotated_keys[:, width:].T, preferred_element_type=jnp.float32
        )
        weights = (masked_softmax(first, visible) - ratio * masked_softmax(second, visible)).astype(
            jnp.bfloat16
        )
        mixed = jnp.dot(weights, value_head, preferred_element_type=jnp.float32)
        scale = lax.rsqrt(jnp.mean(mixed * mixed, axis=-1, keepdims=True) + norm_eps)
        return (mixed * scale * gain).astype(jnp.bfloat16)

    starts = jnp.arange(length // block, dtype=jnp.int32) * block
    return lax.map(one_block, starts).reshape(length, value_head.shape[1])


def on_device(queries, keys, values, mix_ratio, out_gain, out_weight):
    groups = lax.axis_size("sp")
    heads_here = queries.shape[2] // groups
    query_all, key_all, value_all = (
        lax.all_to_all(queries, "sp", split_axis=2, concat_axis=1, tiled=True),
        lax.all_to_all(keys, "sp", split_axis=2, concat_axis=1, tiled=True),
        lax.all_to_all(values, "sp", split_axis=2, concat_axis=1, tiled=True),
    )
    seqs = query_all.shape[0]
    length = query_all.shape[1]
    first_head = lax.axis_index("sp") * heads_here
    ratios = lax.dynamic_slice_in_dim(mix_ratio, first_head, heads_here, 0)
    item_ratios = jnp.tile(ratios, seqs)

    def by_item(field):
        return jnp.swapaxes(field, 1, 2).reshape(seqs * heads_here, length, field.shape[3])

    def one_head(head_items):
        query_head, key_head, value_head, ratio = head_items
        return head_attention(query_head, key_head, value_head, ratio, out_gain)

    heads = lax.map(
        one_head, (by_item(query_all), by_item(key_all), by_item(value_all), item_ratios)
    )
    attended = jnp.swapaxes(heads.reshape(seqs, heads_here, length, heads.shape[2]), 1, 2)
    returned = lax.all_to_all(attended, "sp", split_axis=1, concat_axis=2, tiled=True)
    tokens_here = returned.shape[1]
    token_rows = returned.reshape(seqs * tokens_here, -1)
    result = jnp.dot(
        token_rows,
        lax.all_gather(out_weight, "dp", axis=1, tiled=True),
        preferred_element_type=jnp.float32,
    ).astype(jnp.bfloat16)
    return result.reshape(seqs, tokens_here, -1)


def solution(mesh):
    in_specs = (
        P("dp", "sp", None, None),
        P("dp", "sp", None, None),
        P("dp", "sp", None, None),
        P(),
        P(),
        P(None, "dp"),
    )
    out_specs = P("dp", "sp", None)
    return jax.shard_map(
        on_device, mesh=mesh, in_specs=in_specs, out_specs=out_specs, check_vma=False
    )
```

profile of v0, /device:TPU:0, one launch (start us, length us, event | category | flops | bytes accessed | tf_op | source)
XLA Modules:
  0.0 221.7 jit_solution(10596133892505202635)
XLA Ops:
  6.5 2.2 %copy.37 = bf16[1,192,16,128]{3,1,0,2:T(8,128)(2,1)} copy(bf16[1,192,16,128]{3,2,1,0:T(8,128)(2,1)} %param.10) | data formatting | bytes 1572864 | tf_op args[0]
  8.8 4.2 %all-to-all-start = ((bf16[1,192,16,128]{3,1,0,2:T(8,128)(2,1)}), bf16[1,192,16,128]{3,1,0,2:T(8,128)(2,1)S(1)}, u32[]{:S(2)}, u32[]{:S(2)}) async-start(bf16[1,192,16,128]{3,1,0,2:T(8,128)(2,1)} %copy.37), calls=%async_computation | async-start | bytes 1572864 | tf_op jit(solution)/shard_map/all_to_all | solution.py:69
  13.0 2.2 %copy.40 = bf16[1,192,16,128]{3,1,0,2:T(8,128)(2,1)} copy(bf16[1,192,16,128]{3,2,1,0:T(8,128)(2,1)} %param.11) | data formatting | bytes 1572864 | tf_op args[1]
  15.2 9.3 %all-to-all-done = bf16[1,192,16,128]{3,1,0,2:T(8,128)(2,1)S(1)} async-done(((bf16[1,192,16,128]{3,1,0,2:T(8,128)(2,1)}), bf16[1,192,16,128]{3,1,0,2:T(8,128)(2,1)S(1)}, u32[]{:S(2)}, u32[]{:S(2)}) %all-to-all-start) | async-done | bytes 786464 | tf_op jit(solution)/shard_map/all_to_all | solution.py:69
  24.6 3.5 %all-to-all-start.1 = ((bf16[1,192,16,128]{3,1,0,2:T(8,128)(2,1)}), bf16[1,192,16,128]{3,1,0,2:T(8,128)(2,1)S(1)}, u32[]{:S(2)}, u32[]{:S(2)}) async-start(bf16[1,192,16,128]{3,1,0,2:T(8,128)(2,1)} %copy.40), calls=%async_computation.1 | async-start | bytes 1572864 | tf_op jit(solution)/shard_map/all_to_all | solution.py:70
  28.1 2.3 %copy.43 = bf16[1,192,16,128]{3,1,0,2:T(8,128)(2,1)} copy(bf16[1,192,16,128]{3,2,1,0:T(8,128)(2,1)} %param.12) | data formatting | bytes 1572864 | tf_op args[2]
  30.4 8.2 %all-to-all-done.1 = bf16[1,192,16,128]{3,1,0,2:T(8,128)(2,1)S(1)} async-done(((bf16[1,192,16,128]{3,1,0,2:T(8,128)(2,1)}), bf16[1,192,16,128]{3,1,0,2:T(8,128)(2,1)S(1)}, u32[]{:S(2)}, u32[]{:S(2)}) %all-to-all-start.1) | async-done | bytes 786464 | tf_op jit(solution)/shard_map/all_to_all | solution.py:70
  38.6 3.5 %all-to-all-start.2 = ((bf16[1,192,16,128]{3,1,0,2:T(8,128)(2,1)}), bf16[1,192,16,128]{3,1,0,2:T(8,128)(2,1)S(1)}, u32[]{:S(2)}, u32[]{:S(2)}) async-start(bf16[1,192,16,128]{3,1,0,2:T(8,128)(2,1)} %copy.43), calls=%async_computation.2 | async-start | bytes 1572864 | tf_op jit(solution)/shard_map/all_to_all | solution.py:71
  42.2 0.7 all-gather.2.cloned.1.call-update
  45.3 6.5 %all-to-all-done.2 = bf16[1,192,16,128]{3,1,0,2:T(8,128)(2,1)S(1)} async-done(((bf16[1,192,16,128]{3,1,0,2:T(8,128)(2,1)}), bf16[1,192,16,128]{3,1,0,2:T(8,128)(2,1)S(1)}, u32[]{:S(2)}, u32[]{:S(2)}) %all-to-all-start.2) | async-done | bytes 786464 | tf_op jit(solution)/shard_map/all_to_all | solution.py:71
  51.8 143.6 %while.33 = (s32[]{:T(128)}, bf16[8,384,128]{2,1,0:T(8,128)(2,1)}, bf16[8,384,128]{1,2,0:T(8,128)(2,1)S(1)}, bf16[8,384,128]{1,2,0:T(8,128)(2,1)S(1)}, f32[8]{0:...) while((s32[]{:T(128)}, bf16[8,384,128]{2,1,0:T(8,128)(2,1)}, ...), condition=%wide.region_8.9_spmd, body=%wide.region_0.8_spmd.sunk | while | flops 26882248 | bytes 4764884 | solution.py:86
  53.1 16.0 %while.34 = (s32[]{:T(128)}, bf16[3,128,128]{2,1,0:T(8,128)(2,1)S(1)}, s32[3]{0:T(128)S(1)}, bf16[384,128]{0,1:T(8,128)(2,1)S(1)}, bf16[384,128]{1,0:T(8,128)(2,...) while((s32[]{:T(128)}, ...), condition=%wide.region_7.7_spmd.clone, body=%wide.region_1.6_spmd.clone.sunk | while | flops 26083076 | bytes 1811655 | solution.py:62
  57.2 0.9 multiply_reduce_fusion.2
  62.6 0.9 multiply_reduce_fusion.2
  67.9 0.9 multiply_reduce_fusion.2
  69.1 0.7 bitcast_dynamic-update-slice_fusion.2
  71.1 16.0 %while.34 = (s32[]{:T(128)}, bf16[3,128,128]{2,1,0:T(8,128)(2,1)S(1)}, s32[3]{0:T(128)S(1)}, bf16[384,128]{0,1:T(8,128)(2,1)S(1)}, bf16[384,128]{1,0:T(8,128)(2,...) while((s32[]{:T(128)}, ...), condition=%wide.region_7.7_spmd.clone, body=%wide.region_1.6_spmd.clone.sunk | while | flops 26083076 | bytes 1811655 | solution.py:62
  75.2 0.9 multiply_reduce_fusion.2
  80.5 0.9 multiply_reduce_fusion.2
  85.9 0.9 multiply_reduce_fusion.2
  87.1 0.7 bitcast_dynamic-update-slice_fusion.2
  89.0 16.0 %while.34 = (s32[]{:T(128)}, bf16[3,128,128]{2,1,0:T(8,128)(2,1)S(1)}, s32[3]{0:T(128)S(1)}, bf16[384,128]{0,1:T(8,128)(2,1)S(1)}, bf16[384,128]{1,0:T(8,128)(2,...) while((s32[]{:T(128)}, ...), condition=%wide.region_7.7_spmd.clone, body=%wide.region_1.6_spmd.clone.sunk | while | flops 26083076 | bytes 1811655 | solution.py:62
  93.1 0.9 multiply_reduce_fusion.2
  98.5 0.9 multiply_reduce_fusion.2
  103.8 0.9 multiply_reduce_fusion.2
  107.0 16.0 %while.34 = (s32[]{:T(128)}, bf16[3,128,128]{2,1,0:T(8,128)(2,1)S(1)}, s32[3]{0:T(128)S(1)}, bf16[384,128]{0,1:T(8,128)(2,1)S(1)}, bf16[384,128]{1,0:T(8,128)(2,...) while((s32[]{:T(128)}, ...), condition=%wide.region_7.7_spmd.clone, body=%wide.region_1.6_spmd.clone.sunk | while | flops 26083076 | bytes 1811655 | solution.py:62
  111.1 0.9 multiply_reduce_fusion.2
  116.4 0.9 multiply_reduce_fusion.2
  121.8 1.0 multiply_reduce_fusion.2
  124.9 16.0 %while.34 = (s32[]{:T(128)}, bf16[3,128,128]{2,1,0:T(8,128)(2,1)S(1)}, s32[3]{0:T(128)S(1)}, bf16[384,128]{0,1:T(8,128)(2,1)S(1)}, bf16[384,128]{1,0:T(8,128)(2,...) while((s32[]{:T(128)}, ...), condition=%wide.region_7.7_spmd.clone, body=%wide.region_1.6_spmd.clone.sunk | while | flops 26083076 | bytes 1811655 | solution.py:62
  129.0 0.9 multiply_reduce_fusion.2
  134.4 0.9 multiply_reduce_fusion.2
  139.7 0.9 multiply_reduce_fusion.2
  142.8 16.0 %while.34 = (s32[]{:T(128)}, bf16[3,128,128]{2,1,0:T(8,128)(2,1)S(1)}, s32[3]{0:T(128)S(1)}, bf16[384,128]{0,1:T(8,128)(2,1)S(1)}, bf16[384,128]{1,0:T(8,128)(2,...) while((s32[]{:T(128)}, ...), condition=%wide.region_7.7_spmd.clone, body=%wide.region_1.6_spmd.clone.sunk | while | flops 26083076 | bytes 1811655 | solution.py:62
  147.0 0.9 multiply_reduce_fusion.2
  152.3 0.9 multiply_reduce_fusion.2
  157.7 0.9 multiply_reduce_fusion.2
  160.8 16.0 %while.34 = (s32[]{:T(128)}, bf16[3,128,128]{2,1,0:T(8,128)(2,1)S(1)}, s32[3]{0:T(128)S(1)}, bf16[384,128]{0,1:T(8,128)(2,1)S(1)}, bf16[384,128]{1,0:T(8,128)(2,...) while((s32[]{:T(128)}, ...), condition=%wide.region_7.7_spmd.clone, body=%wide.region_1.6_spmd.clone.sunk | while | flops 26083076 | bytes 1811655 | solution.py:62
  164.9 0.9 multiply_reduce_fusion.2
  170.3 0.9 multiply_reduce_fusion.2
  175.6 0.9 multiply_reduce_fusion.2
  178.7 16.0 %while.34 = (s32[]{:T(128)}, bf16[3,128,128]{2,1,0:T(8,128)(2,1)S(1)}, s32[3]{0:T(128)S(1)}, bf16[384,128]{0,1:T(8,128)(2,1)S(1)}, bf16[384,128]{1,0:T(8,128)(2,...) while((s32[]{:T(128)}, ...), condition=%wide.region_7.7_spmd.clone, body=%wide.region_1.6_spmd.clone.sunk | while | flops 26083076 | bytes 1811655 | solution.py:62
  182.9 0.9 multiply_reduce_fusion.2
  188.2 0.9 multiply_reduce_fusion.2
  193.6 0.9 multiply_reduce_fusion.2
  195.4 1.6 copy.59
  197.1 11.2 %all_to_all.69 = bf16[1,384,8,128]{3,2,0,1:T(8,128)(2,1)S(1)} all-to-all(bf16[1,384,8,128]{3,2,0,1:T(8,128)(2,1)S(1)} %bitcast.88), channel_id=1, replica_groups=mesh['sp'=2,'dp'=16] {'sp'}, dimensions={1} | all-to-all | bytes 1572864 | tf_op jit(solution)/shard_map/all_to_all | solution.py:90
  208.8 6.1 %fusion.12 = bf16[1,192,2048]{2,1,0:T(8,128)(2,1)} fusion(bf16[192,2048]{1,0:T(8,128)(2,1)S(1)} %reshape.130, bf16[2048,2048]{1,0:T(8,128)(2,1)} %all-gather.2.cloned.1.call-done), kind=kOutput, calls=%fused_computation.38 | convolution fusion | flops 1611005952 | bytes 9961472 | tf_op jit(solution)/shard_map/dot_general | solution.py:93
  (351 shorter events, 75.0 us)
Async XLA Ops:
  6.5 36.4 %copy-start.1 = (f32[16]{0:T(128)S(1)}, f32[16]{0:T(128)}, u32[]{:S(2)}) copy-start(f32[16]{0:T(128)} %param.13) | copy-start | bytes 196
  8.8 15.8 %all-to-all-start = ((bf16[1,192,16,128]{3,1,0,2:T(8,128)(2,1)}), bf16[1,192,16,128]{3,1,0,2:T(8,128)(2,1)S(1)}, u32[]{:S(2)}, u32[]{:S(2)}) async-start(bf16[1,192,16,128]{3,1,0,2:T(8,128)(2,1)} %copy.37), calls=%async_computation | async-start | bytes 1572864 | tf_op jit(solution)/shard_map/all_to_all | solution.py:69
  15.2 36.6 %copy-start = (f32[128]{0:T(128)S(1)}, f32[128]{0:T(128)}, u32[]{:S(2)}) copy-start(f32[128]{0:T(128)} %param.14) | copy-start | bytes 1540
  24.6 14.0 %all-to-all-start.1 = ((bf16[1,192,16,128]{3,1,0,2:T(8,128)(2,1)}), bf16[1,192,16,128]{3,1,0,2:T(8,128)(2,1)S(1)}, u32[]{:S(2)}, u32[]{:S(2)}) async-start(bf16[1,192,16,128]{3,1,0,2:T(8,128)(2,1)} %copy.40), calls=%async_computation.1 | async-start | bytes 1572864 | tf_op jit(solution)/shard_map/all_to_all | solution.py:70
  38.6 13.2 %all-to-all-start.2 = ((bf16[1,192,16,128]{3,1,0,2:T(8,128)(2,1)}), bf16[1,192,16,128]{3,1,0,2:T(8,128)(2,1)S(1)}, u32[]{:S(2)}, u32[]{:S(2)}) async-start(bf16[1,192,16,128]{3,1,0,2:T(8,128)(2,1)} %copy.43), calls=%async_computation.2 | async-start | bytes 1572864 | tf_op jit(solution)/shard_map/all_to_all | solution.py:71
  42.1 166.6 %all-gather.2.cloned.1.call-start = ((), (), s32[]{:S(2)}) async-start(), calls=%async_computation.4 | async-start | bytes 8912896 | tf_op jit(solution)/shard_map/all_gather | solution.py:95
Sparse Core Ops, SparseCore 0:
  45.1 79.5 all-gather.1
where the time goes:
time: 223 us; the launch traced here: 222 us
  loops' own time  47.4 us (21%)
  matrix products  47.1 us (21%)
  local copies, waits for them, and re-layouts  40.5 us (18%)
  other arithmetic  25.9 us (12%)
  waiting for transfers between devices  24.8 us (11%)
  between operations  13.5 us (6%)
  starting transfers between devices  11.3 us (5%)
  blocking collectives  11.2 us (5%)
    another operation x8, loops' own time, head_attention(): return lax.map(one_block, starts).reshape(length, value_head.shape[1])  46.7 us
    dot_general x24, matrix products, one_block(): mixed = jnp.dot(weights, value_head, preferred_element_type=jnp.float32)  22.8 us
    add x24, other arithmetic, one_block(): start + jnp.arange(block, dtype=jnp.int32)  15.2 us
    dynamic_slice x24, local copies, waits for them, and re-layouts, head_attention(): return lax.map(one_block, starts).reshape(length, value_head.shape[1])  14.6 us
    all_to_all x1, blocking collectives, on_device(): lax.all_to_all(attended, 'sp', split_axis=1, concat_axis=2, tiled=True)  11.2 us
    all_to_all x1, waiting for transfers between devices, on_device(): lax.all_to_all(queries, 'sp', split_axis=2, concat_axis=1, tiled=True)  9.35 us
    dot_general x24, matrix products, one_block(): jnp.dot(query_rows[:, width:], rotated_keys[:, width:].T, preferred_eleme...  9.13 us
    dot_general x24, matrix products, one_block(): jnp.dot(query_rows[:, :width], rotated_keys[:, :width].T, preferred_eleme...  9.12 us
  transfers between devices with their start and end apart: 4, of which 3 were waited for; matrix products, arithmetic and copies ran while one was open for 47% of the time, Pallas kernels for 0%

commit v1 on v0

--- a/solution.py
+++ b/solution.py
@@ -65,8 +65,17 @@
 def on_device(queries, keys, values, mix_ratio, out_gain, out_weight):
     groups = lax.axis_size("sp")
     heads_here = queries.shape[2] // groups
+    _enter_ladders = lambda piece_in: jnp.concatenate(
+        lax.all_to_all(
+            jnp.stack(jnp.split(piece_in, lax.psum(1, axis_name="sp"), axis=2)),
+            axis_name="sp",
+            split_axis=0,
+            concat_axis=0,
+        ),
+        axis=1,
+    )
     query_all, key_all, value_all = (
-        lax.all_to_all(queries, "sp", split_axis=2, concat_axis=1, tiled=True),
+        _enter_ladders(queries),
         lax.all_to_all(keys, "sp", split_axis=2, concat_axis=1, tiled=True),
         lax.all_to_all(values, "sp", split_axis=2, concat_axis=1, tiled=True),
     )

time: 223 us -> 230 us (1.031)
  local copies, waits for them, and re-layouts: 40.5 us -> 45.6 us
    dynamic_slice x16, local copies, waits for them, and re-layouts: 5.33 us -> 12.6 us  [on_device(): lax.map(one_head, (by_item(query_all), by_item(key_all), by_item(value_al...]
    unnamed x7 -> x8, local copies, waits for them, and re-layouts: 6.74 us -> 3.3 us
  transfers between devices with their start and end apart: 4 -> 4, of which waited for: 3 -> 3; matrix products, arithmetic and copies ran while one was open for 47% -> 49% of each run, Pallas kernels for 0% -> 0%
where the time goes in v1:
time: 230 us; the launch traced here: 229 us
  matrix products  48.4 us (21%)
  loops' own time  46.3 us (20%)
  local copies, waits for them, and re-layouts  45.6 us (20%)
  other arithmetic  26.6 us (12%)
  waiting for transfers between devices  25.7 us (11%)
  between operations  13.5 us (6%)
  starting transfers between devices  11.5 us (5%)
  blocking collectives  11.2 us (5%)
    another operation x8, loops' own time, head_attention(): return lax.map(one_block, starts).reshape(length, value_head.shape[1])  45.6 us
    dot_general x24, matrix products, one_block(): mixed = jnp.dot(weights, value_head, preferred_element_type=jnp.float32)  24.1 us
    add x24, other arithmetic, one_block(): start + jnp.arange(block, dtype=jnp.int32)  14.9 us
    dynamic_slice x24, local copies, waits for them, and re-layouts, head_attention(): return lax.map(one_block, starts).reshape(length, value_head.shape[1])  14.3 us
    dynamic_slice x16, local copies, waits for them, and re-layouts, on_device(): lax.map(one_head, (by_item(query_all), by_item(key_all), by_item(value_al...  12.6 us
    all_to_all x1, blocking collectives, on_device(): lax.all_to_all(attended, 'sp', split_axis=1, concat_axis=2, tiled=True)  11.2 us
    all_to_all x1, waiting for transfers between devices, on_device(): lax.all_to_all(keys, 'sp', split_axis=2, concat_axis=1, tiled=True)  9.39 us
    all_to_all x1, waiting for transfers between devices, on_device(): lax.all_to_all(jnp.stack(jnp.split(piece_in, lax.psum(1, axis_name='sp'),...  9.36 us
  transfers between devices with their start and end apart: 4, of which 3 were waited for; matrix products, arithmetic and copies ran while one was open for 49% of the time, Pallas kernels for 0%

profile of v1, /device:TPU:0, one launch (start us, length us, event | category | flops | bytes accessed | tf_op | source)
XLA Modules:
  0.0 228.7 jit_solution(8788406123953936512)
XLA Ops:
  6.5 1.2 slice_bitcast_fusion.1
  7.8 0.9 pad_maximum_fusion.1
  8.7 4.4 %all-to-all-start = ((bf16[2,1,192,8,128]{4,3,2,1,0:T(8,128)(2,1)}), bf16[2,1,192,8,128]{4,3,2,1,0:T(8,128)(2,1)S(1)}, u32[]{:S(2)}, u32[]{:S(2)}) async-start(bf16[2,1,192,8,128]{4,3,2,1,0:T(8,128)(2,1)} %pad_maximum_fusion.1), calls=%async_computation | async-start | bytes 1572864 | tf_op jit(solution)/shard_map/all_to_all | solution.py:69
  13.1 2.2 copy.36
  15.3 9.4 %all-to-all-done = bf16[2,1,192,8,128]{4,3,2,1,0:T(8,128)(2,1)S(1)} async-done(((bf16[2,1,192,8,128]{4,3,2,1,0:T(8,128)(2,1)}), bf16[2,1,192,8,128]{4,3,2,1,0:T(8,128)(2,1)S(1)}, u32[]{:S(2)}, u32[]{:S(2)}) %all-to-all-start) | async-done | bytes 786464 | tf_op jit(solution)/shard_map/all_to_all | solution.py:69
  24.7 3.5 %all-to-all-start.1 = ((bf16[1,192,16,128]{3,1,0,2:T(8,128)(2,1)}), bf16[1,192,16,128]{3,1,0,2:T(8,128)(2,1)S(1)}, u32[]{:S(2)}, u32[]{:S(2)}) async-start(bf16[1,192,16,128]{3,1,0,2:T(8,128)(2,1)} %copy.36), calls=%async_computation.1 | async-start | bytes 1572864 | tf_op jit(solution)/shard_map/all_to_all | solution.py:79
  28.2 1.1 copy.39
  29.3 9.4 %all-to-all-done.1 = bf16[1,192,16,128]{3,1,0,2:T(8,128)(2,1)S(1)} async-done(((bf16[1,192,16,128]{3,1,0,2:T(8,128)(2,1)}), bf16[1,192,16,128]{3,1,0,2:T(8,128)(2,1)S(1)}, u32[]{:S(2)}, u32[]{:S(2)}) %all-to-all-start.1) | async-done | bytes 786464 | tf_op jit(solution)/shard_map/all_to_all | solution.py:79
  38.7 3.5 %all-to-all-start.2 = ((bf16[1,192,16,128]{3,1,0,2:T(8,128)(2,1)}), bf16[1,192,16,128]{3,1,0,2:T(8,128)(2,1)S(1)}, u32[]{:S(2)}, u32[]{:S(2)}) async-start(bf16[1,192,16,128]{3,1,0,2:T(8,128)(2,1)} %copy.39), calls=%async_computation.2 | async-start | bytes 1572864 | tf_op jit(solution)/shard_map/all_to_all | solution.py:80
  44.2 1.4 copy.42
  45.7 6.2 %all-to-all-done.2 = bf16[1,192,16,128]{3,1,0,2:T(8,128)(2,1)S(1)} async-done(((bf16[1,192,16,128]{3,1,0,2:T(8,128)(2,1)}), bf16[1,192,16,128]{3,1,0,2:T(8,128)(2,1)S(1)}, u32[]{:S(2)}, u32[]{:S(2)}) %all-to-all-start.2) | async-done | bytes 786464 | tf_op jit(solution)/shard_map/all_to_all | solution.py:80
  51.9 150.5 %while.33 = (s32[]{:T(128)}, bf16[8,384,128]{2,1,0:T(8,128)(2,1)}, bf16[8,384,128]{1,2,0:T(8,128)(2,1)S(1)}, bf16[8,384,128]{1,2,0:T(8,128)(2,1)}, f32[8]{0:T(12...) while((s32[]{:T(128)}, bf16[8,384,128]{2,1,0:T(8,128)(2,1)}, ...), condition=%wide.region_8.9_spmd, body=%wide.region_0.8_spmd.sunk | while | flops 26882248 | bytes 4764884 | solution.py:95
  51.9 0.9 constant_dynamic-slice_fusion.3
  54.1 16.0 %while.34 = (s32[]{:T(128)}, bf16[3,128,128]{2,1,0:T(8,128)(2,1)S(1)}, s32[3]{0:T(128)S(1)}, bf16[384,128]{0,1:T(8,128)(2,1)S(1)}, bf16[384,128]{1,0:T(8,128)(2,...) while((s32[]{:T(128)}, ...), condition=%wide.region_7.7_spmd.clone, body=%wide.region_1.6_spmd.clone.sunk | while | flops 26083076 | bytes 1811655 | solution.py:62
  58.2 1.0 multiply_reduce_fusion.2
  63.5 1.0 multiply_reduce_fusion.2
  68.8 1.0 multiply_reduce_fusion.2
  72.9 16.0 %while.34 = (s32[]{:T(128)}, bf16[3,128,128]{2,1,0:T(8,128)(2,1)S(1)}, s32[3]{0:T(128)S(1)}, bf16[384,128]{0,1:T(8,128)(2,1)S(1)}, bf16[384,128]{1,0:T(8,128)(2,...) while((s32[]{:T(128)}, ...), condition=%wide.region_7.7_spmd.clone, body=%wide.region_1.6_spmd.clone.sunk | while | flops 26083076 | bytes 1811655 | solution.py:62
  77.0 1.0 multiply_reduce_fusion.2
  82.3 1.0 multiply_reduce_fusion.2
  87.6 1.0 multiply_reduce_fusion.2
  91.7 16.0 %while.34 = (s32[]{:T(128)}, bf16[3,128,128]{2,1,0:T(8,128)(2,1)S(1)}, s32[3]{0:T(128)S(1)}, bf16[384,128]{0,1:T(8,128)(2,1)S(1)}, bf16[384,128]{1,0:T(8,128)(2,...) while((s32[]{:T(128)}, ...), condition=%wide.region_7.7_spmd.clone, body=%wide.region_1.6_spmd.clone.sunk | while | flops 26083076 | bytes 1811655 | solution.py:62
  95.8 1.0 multiply_reduce_fusion.2
  101.1 1.0 multiply_reduce_fusion.2
  106.4 1.0 multiply_reduce_fusion.2
  110.5 16.0 %while.34 = (s32[]{:T(128)}, bf16[3,128,128]{2,1,0:T(8,128)(2,1)S(1)}, s32[3]{0:T(128)S(1)}, bf16[384,128]{0,1:T(8,128)(2,1)S(1)}, bf16[384,128]{1,0:T(8,128)(2,...) while((s32[]{:T(128)}, ...), condition=%wide.region_7.7_spmd.clone, body=%wide.region_1.6_spmd.clone.sunk | while | flops 26083076 | bytes 1811655 | solution.py:62
  114.6 1.0 multiply_reduce_fusion.2
  119.9 1.0 multiply_reduce_fusion.2
  125.3 1.0 multiply_reduce_fusion.2
  129.3 16.0 %while.34 = (s32[]{:T(128)}, bf16[3,128,128]{2,1,0:T(8,128)(2,1)S(1)}, s32[3]{0:T(128)S(1)}, bf16[384,128]{0,1:T(8,128)(2,1)S(1)}, bf16[384,128]{1,0:T(8,128)(2,...) while((s32[]{:T(128)}, ...), condition=%wide.region_7.7_spmd.clone, body=%wide.region_1.6_spmd.clone.sunk | while | flops 26083076 | bytes 1811655 | solution.py:62
  133.4 1.0 multiply_reduce_fusion.2
  138.7 1.0 multiply_reduce_fusion.2
  144.1 1.0 multiply_reduce_fusion.2
  148.1 16.0 %while.34 = (s32[]{:T(128)}, bf16[3,128,128]{2,1,0:T(8,128)(2,1)S(1)}, s32[3]{0:T(128)S(1)}, bf16[384,128]{0,1:T(8,128)(2,1)S(1)}, bf16[384,128]{1,0:T(8,128)(2,...) while((s32[]{:T(128)}, ...), condition=%wide.region_7.7_spmd.clone, body=%wide.region_1.6_spmd.clone.sunk | while | flops 26083076 | bytes 1811655 | solution.py:62
  152.2 1.0 multiply_reduce_fusion.2
  157.5 1.0 multiply_reduce_fusion.2
  162.9 1.0 multiply_reduce_fusion.2
  166.9 16.0 %while.34 = (s32[]{:T(128)}, bf16[3,128,128]{2,1,0:T(8,128)(2,1)S(1)}, s32[3]{0:T(128)S(1)}, bf16[384,128]{0,1:T(8,128)(2,1)S(1)}, bf16[384,128]{1,0:T(8,128)(2,...) while((s32[]{:T(128)}, ...), condition=%wide.region_7.7_spmd.clone, body=%wide.region_1.6_spmd.clone.sunk | while | flops 26083076 | bytes 1811655 | solution.py:62
  171.0 1.0 multiply_reduce_fusion.2
  176.3 1.0 multiply_reduce_fusion.2
  181.7 1.0 multiply_reduce_fusion.2
  185.8 16.0 %while.34 = (s32[]{:T(128)}, bf16[3,128,128]{2,1,0:T(8,128)(2,1)S(1)}, s32[3]{0:T(128)S(1)}, bf16[384,128]{0,1:T(8,128)(2,1)S(1)}, bf16[384,128]{1,0:T(8,128)(2,...) while((s32[]{:T(128)}, ...), condition=%wide.region_7.7_spmd.clone, body=%wide.region_1.6_spmd.clone.sunk | while | flops 26083076 | bytes 1811655 | solution.py:62
  189.8 1.0 multiply_reduce_fusion.2
  195.1 1.0 multiply_reduce_fusion.2
  200.5 1.0 multiply_reduce_fusion.2
  202.4 1.6 copy.54
  204.0 11.2 %all_to_all.56 = bf16[1,384,8,128]{3,2,0,1:T(8,128)(2,1)S(1)} all-to-all(bf16[1,384,8,128]{3,2,0,1:T(8,128)(2,1)S(1)} %bitcast.86), channel_id=1, replica_groups=mesh['sp'=2,'dp'=16] {'sp'}, dimensions={1} | all-to-all | bytes 1572864 | tf_op jit(solution)/shard_map/all_to_all | solution.py:99
  215.8 6.1 %fusion.12 = bf16[1,192,2048]{2,1,0:T(8,128)(2,1)} fusion(bf16[192,2048]{1,0:T(8,128)(2,1)S(1)} %reshape.134, bf16[2048,2048]{1,0:T(8,128)(2,1)} %all-gather.2.cloned.1.call-done), kind=kOutput, calls=%fused_computation.38 | convolution fusion | flops 1611005952 | bytes 9961472 | tf_op jit(solution)/shard_map/dot_general | solution.py:102
  (352 shorter events, 81.6 us)
Async XLA Ops:
  6.5 21.7 %copy-start = (bf16[1,192,16,128]{3,2,1,0:T(8,128)(2,1)S(1)}, bf16[1,192,16,128]{3,2,1,0:T(8,128)(2,1)}, u32[]{:S(2)}) copy-start(bf16[1,192,16,128]{3,2,1,0:T(8,128)(2,1)} %param.12) | copy-start | bytes 2359300
  6.5 36.5 %copy-start.2 = (f32[16]{0:T(128)S(1)}, f32[16]{0:T(128)}, u32[]{:S(2)}) copy-start(f32[16]{0:T(128)} %param.13) | copy-start | bytes 196
  8.7 43.2 %copy-start.1 = (f32[128]{0:T(128)S(1)}, f32[128]{0:T(128)}, u32[]{:S(2)}) copy-start(f32[128]{0:T(128)} %param.14) | copy-start | bytes 1540
  8.7 15.9 %all-to-all-start = ((bf16[2,1,192,8,128]{4,3,2,1,0:T(8,128)(2,1)}), bf16[2,1,192,8,128]{4,3,2,1,0:T(8,128)(2,1)S(1)}, u32[]{:S(2)}, u32[]{:S(2)}) async-start(bf16[2,1,192,8,128]{4,3,2,1,0:T(8,128)(2,1)} %pad_maximum_fusion.1), calls=%async_computation | async-start | bytes 1572864 | tf_op jit(solution)/shard_map/all_to_all | solution.py:69
  24.7 14.0 %all-to-all-start.1 = ((bf16[1,192,16,128]{3,1,0,2:T(8,128)(2,1)}), bf16[1,192,16,128]{3,1,0,2:T(8,128)(2,1)S(1)}, u32[]{:S(2)}, u32[]{:S(2)}) async-start(bf16[1,192,16,128]{3,1,0,2:T(8,128)(2,1)} %copy.36), calls=%async_computation.1 | async-start | bytes 1572864 | tf_op jit(solution)/shard_map/all_to_all | solution.py:79
  38.7 13.2 %all-to-all-start.2 = ((bf16[1,192,16,128]{3,1,0,2:T(8,128)(2,1)}), bf16[1,192,16,128]{3,1,0,2:T(8,128)(2,1)S(1)}, u32[]{:S(2)}, u32[]{:S(2)}) async-start(bf16[1,192,16,128]{3,1,0,2:T(8,128)(2,1)} %copy.39), calls=%async_computation.2 | async-start | bytes 1572864 | tf_op jit(solution)/shard_map/all_to_all | solution.py:80
  42.2 173.5 %all-gather.2.cloned.1.call-start = ((), (), s32[]{:S(2)}) async-start(), calls=%async_computation.4 | async-start | bytes 8912896 | tf_op jit(solution)/shard_map/all_gather | solution.py:104
Sparse Core Ops, SparseCore 0:
  45.2 79.3 all-gather.1
